TPU v7x, 32 devices: a whole 2x2x4 slice. The times are simulated.
32 devices in a mesh: sp: 4 (over z), tp: 4 (over y, x), dp: 2 (over core).
Axes of the slice: x: 2, y: 2, z: 4, core: 2. Of those that a mesh axis runs over, the one named last changes fastest.
Arguments:
- latent: bfloat16 [2, 4096, 2048], P('dp', 'sp'), may hold values from -4 to 4
- context: bfloat16 [2, 768, 2048], P('dp', 'sp'), may hold values from -6 to 6
- cond: float32 [2, 2048], P('dp'), may hold values from -6 to 6
- ctx_cond: float32 [2048], replicated, may hold values from -6 to 6
- norm_gain: float32 [2048], replicated, may hold values from 0.1 to 1.9
- mod_shift: bfloat16 [2048, 2048], P('sp', 'tp'), may hold values from -0.125 to 0.125
- mod_scale: bfloat16 [2048, 2048], P('sp', 'tp'), may hold values from -0.125 to 0.125
- mod_gate: bfloat16 [2048, 2048], P('sp', 'tp'), may hold values from -0.125 to 0.125
- w_query: bfloat16 [2048, 2048], P(None, 'tp'), may hold values from -0.125 to 0.125
- w_key: bfloat16 [2048, 512], P(None, 'tp'), may hold values from -0.125 to 0.125
- w_value: bfloat16 [2048, 512], P(None, 'tp'), may hold values from -0.125 to 0.125
- w_out: bfloat16 [2048, 2048], P('tp'), may hold values from -2 to 2
- q_gain: float32 [128], replicated, may hold values from 0.1 to 1.9
- k_gain: float32 [128], replicated, may hold values from 0.1 to 1.9
- sinks: float32 [16], P('tp'), may hold values from 3 to 8
Outputs:
- result: bfloat16 [2, 4096, 2048], P('dp', ('sp', 'tp'))
All inputs are finite; a program needn't handle non-finite values.
Results may differ from a plain program's by a relative error of at most 0.013.
Values may be sent and summed in bfloat16 or wider, within the bound.
A program may use at most 128 MiB of HBM per device.

v0:
```python
import jax
import jax.numpy as jnp
from jax import lax
from jax.sharding import PartitionSpec as P

HEAD_DIM = 128
WINDOW = 128
GRID_W = 64


NORM_EPSILON = 1e-06
ROPE_BASE = 10000.0


def extended(array, sides, width):
    for axis, dim in sides:
        peers, length = (lax.axis_size(axis), array.shape[dim])
        up = [(i, (i + 1) % peers) for i in range(peers - 1)]
        down = [(j, i) for i, j in up]
        last = lax.slice_in_dim(array, length - width, length, axis=dim)
        first = lax.slice_in_dim(array, 0, width, axis=dim)
        before = lax.ppermute(last, axis, up)
        after = lax.ppermute(first, axis, down)
        array = jnp.concatenate([before, array, after], axis=dim)
    return array


def head_norm(vectors, gain_row):
    return (
        vectors
        * lax.rsqrt(jnp.mean(vectors * vectors, axis=-1, keepdims=True) + NORM_EPSILON)
        * gain_row
    )


def modulated(rows_in, gain_row, shift_row, scale_row):
    values = rows_in.astype(jnp.float32)
    normed = (
        values
        * lax.rsqrt(jnp.mean(values * values, axis=-1, keepdims=True) + NORM_EPSILON)
        * gain_row
    )
    return (normed * (1.0 + scale_row) + shift_row).astype(jnp.bfloat16)


def rotate_half(halves, coords):
    quarter = halves.shape[-1] // 2
    frequency = ROPE_BASE ** (-jnp.arange(quarter, dtype=jnp.float32) / quarter)
    angles = coords.astype(jnp.float32)[:, None] * frequency
    cosine_part = jnp.cos(angles)[:, None, :]
    sine_part = jnp.sin(angles)[:, None, :]
    first_part = halves[..., :quarter]
    second_part = halves[..., quarter:]
    return jnp.concatenate(
        [
            first_part * cosine_part - second_part * sine_part,
            second_part * cosine_part + first_part * sine_part,
        ],
        axis=-1,
    )


def rotate(vectors, positions):
    half_dim = vectors.shape[-1] // 2
    return jnp.concatenate(
        [
            rotate_half(vectors[..., :half_dim], positions // GRID_W),
            rotate_half(vectors[..., half_dim:], positions % GRID_W),
        ],
        axis=-1,
    )


def per_device(
    latent,
    context,
    cond,
    ctx_cond,
    norm_gain,
    mod_shift,
    mod_scale,
    mod_gate,
    w_query,
    w_key,
    w_value,
    w_out,
    q_gain,
    k_gain,
    sinks,
):
    tok_count = latent.shape[1]
    part_rows = mod_shift.shape[0]
    sp_index = lax.axis_index("sp")
    tp_index = lax.axis_index("tp")
    cond_rows = jnp.stack([cond[0], ctx_cond])
    own_cond = lax.dynamic_slice_in_dim(cond_rows, sp_index * part_rows, part_rows, 1)
    active = jax.nn.silu(own_cond).astype(jnp.bfloat16)
    shifts = jnp.dot(active, mod_shift, preferred_element_type=jnp.float32)
    scales = jnp.dot(active, mod_scale, preferred_element_type=jnp.float32)
    gate_rows = jnp.dot(active[0:1], mod_gate, preferred_element_type=jnp.float32)
    partial_value = jnp.concatenate([shifts, scales, gate_rows], axis=0)
    summed = lax.psum(partial_value, "sp")
    modulation = lax.all_gather(summed, "tp", axis=1, tiled=True)
    lat_in = modulated(latent[0], norm_gain, modulation[0], modulation[2])
    ctx_in = modulated(context[0], norm_gain, modulation[1], modulation[3])
    gate_row = modulation[4]
    kv_local = w_key.shape[1] // HEAD_DIM
    q_local = w_query.shape[1] // HEAD_DIM
    group_size = q_local // kv_local
    kv_width = kv_local * HEAD_DIM
    score_scale = HEAD_DIM ** (-0.5)
    positions = sp_index * tok_count + jnp.arange(tok_count, dtype=jnp.int32)
    lat_queries = rotate(
        head_norm(
            jnp.dot(lat_in, w_query, preferred_element_type=jnp.float32).reshape(
                tok_count, q_local, HEAD_DIM
            ),
            q_gain,
        ),
        positions,
    ).astype(jnp.bfloat16)
    lat_keys = rotate(
        head_norm(
            jnp.dot(lat_in, w_key, preferred_element_type=jnp.float32).reshape(
                tok_count, kv_local, HEAD_DIM
            ),
            k_gain,
        ),
        positions,
    ).astype(jnp.bfloat16)
    lat_values = jnp.dot(lat_in, w_value, preferred_element_type=jnp.float32).astype(jnp.bfloat16)
    lat_both = jnp.concatenate([lat_keys.reshape(tok_count, kv_width), lat_values], axis=1)
    padded = extended(lat_both, (("sp", 0),), WINDOW)
    piece_keys = head_norm(
        jnp.dot(ctx_in, w_key, preferred_element_type=jnp.float32).reshape(
            ctx_in.shape[0], kv_local, HEAD_DIM
        ),
        k_gain,
    ).astype(jnp.bfloat16)
    piece_values = jnp.dot(ctx_in, w_value, preferred_element_type=jnp.float32).astype(jnp.bfloat16)
    context_both = lax.all_gather(
        jnp.concatenate([piece_keys.reshape(ctx_in.shape[0], kv_width), piece_values], axis=1),
        "sp",
        axis=0,
        tiled=True,
    )
    ctx_count = context_both.shape[0]
    ctx_keys = context_both[:, :kv_width].reshape(ctx_count, kv_local, HEAD_DIM)
    ctx_values = context_both[:, kv_width:].reshape(ctx_count, kv_local, HEAD_DIM)
    block_count = tok_count // WINDOW
    padded_blocks = padded.reshape(block_count + 2, WINDOW, 2 * kv_width)
    window_both = jnp.concatenate(
        [
            padded_blocks[0:block_count],
            padded_blocks[1 : block_count + 1],
            padded_blocks[2 : block_count + 2],
        ],
        axis=1,
    )
    window_keys = window_both[..., :kv_width].reshape(block_count, 3 * WINDOW, kv_local, HEAD_DIM)
    window_values = window_both[..., kv_width:].reshape(block_count, 3 * WINDOW, kv_local, HEAD_DIM)
    query_blocks = lat_queries.reshape(block_count, WINDOW, kv_local, group_size, HEAD_DIM)
    key_rows = jnp.arange(3 * WINDOW, dtype=jnp.int32)
    query_rows = jnp.arange(WINDOW, dtype=jnp.int32)
    offset_rows = key_rows[None, :] - query_rows[:, None]
    in_band = (offset_rows >= 0) & (offset_rows <= 2 * WINDOW)
    key_pos = (
        sp_index * tok_count
        - WINDOW
        + jnp.arange(block_count, dtype=jnp.int32)[:, None] * WINDOW
        + key_rows[None, :]
    )
    seq_total = tok_count * lax.axis_size("sp")
    in_range = (key_pos >= 0) & (key_pos < seq_total)
    in_window = in_band[None, :, :] & in_range[:, None, :]
    scores = (
        jnp.einsum(
            "nqhgd,nkhd->hgnqk", query_blocks, window_keys, preferred_element_type=jnp.float32
        )
        * score_scale
    )
    weights = jnp.where(in_window[None, None], jnp.exp(scores), 0.0)
    flat_queries = lat_queries.reshape(tok_count, kv_local, group_size, HEAD_DIM)
    ctx_weights = jnp.exp(
        jnp.einsum("thgd,chd->hgtc", flat_queries, ctx_keys, preferred_element_type=jnp.float32)
        * score_scale
    )
    sink_exp = jnp.exp(sinks).reshape(kv_local, group_size)
    denominator = (
        jnp.sum(weights, axis=-1).reshape(kv_local, group_size, tok_count)
        + jnp.sum(ctx_weights, axis=-1)
        + sink_exp[:, :, None]
    )
    local_probs = (
        weights / denominator.reshape(kv_local, group_size, block_count, WINDOW)[..., None]
    ).astype(jnp.bfloat16)
    ctx_probs = (ctx_weights / denominator[..., None]).astype(jnp.bfloat16)
    local_part = jnp.einsum(
        "hgnqk,nkhd->nqhgd", local_probs, window_values, preferred_element_type=jnp.float32
    )
    ctx_part = jnp.einsum(
        "hgtc,chd->thgd", ctx_probs, ctx_values, preferred_element_type=jnp.float32
    )
    attended = (local_part.reshape(tok_count, kv_local, group_size, HEAD_DIM) + ctx_part).astype(
        jnp.bfloat16
    )
    attended = attended.reshape(tok_count, q_local * HEAD_DIM)
    sub_rows = tok_count // lax.axis_size("tp")
    mixed_rows = lax.psum_scatter(
        jnp.dot(attended, w_out, preferred_element_type=jnp.float32).astype(jnp.bfloat16),
        "tp",
        scatter_dimension=0,
        tiled=True,
    ).astype(jnp.float32)
    own_rows = lax.dynamic_slice_in_dim(latent[0], tp_index * sub_rows, sub_rows, 0).astype(
        jnp.float32
    )
    result = (own_rows + gate_row * mixed_rows).astype(jnp.bfloat16)
    return result[None]


def solution(mesh):
    in_specs = (
        P("dp", "sp", None),
        P("dp", "sp", None),
        P("dp", None),
        P(),
        P(),
        P("sp", "tp"),
        P("sp", "tp"),
        P("sp", "tp"),
        P(None, "tp"),
        P(None, "tp"),
        P(None, "tp"),
        P("tp", None),
        P(),
        P(),
        P("tp"),
    )
    out_specs = P("dp", ("sp", "tp"), None)
    return jax.shard_map(
        per_device, mesh=mesh, in_specs=in_specs, out_specs=out_specs, check_vma=False
    )
```

profile of v0, /device:TPU:0, one launch (start us, length us, event | category | flops | bytes accessed | tf_op | source)
XLA Modules:
  0.0 197.5 jit_solution(17121578657694832713)
XLA Ops:
  7.6 1.2 fusion.96
  8.8 1.2 fusion.105
  10.0 1.2 fusion.104
  11.2 3.1 %fusion.3 = f32[1024]{0:T(1024)S(1)} fusion(bf16[1,1024,2048]{2,1,0:T(8,128)(2,1)} %param.15), kind=kLoop, calls=%fused_computation.8 | loop fusion | flops 6290432 | bytes 4198400 | tf_op jit(solution)/shard_map/reduce_sum | solution.py:40
  14.3 20.5 %psum.7 = f32[5,512]{1,0:T(8,128)S(1)} all-reduce(f32[5,512]{1,0:T(8,128)S(1)} %pad_maximum_fusion.4), channel_id=1, replica_groups=mesh['sp'=4,'tp'=4,'dp'=2] {'sp'}, use_global_device_ids=true, to_apply=%region_0.1 | all-reduce | flops 2560 | bytes 20480 | tf_op jit(solution)/shard_map/psum | solution.py:102
  34.8 8.2 %all_gather.6 = f32[5,2048]{1,0:T(8,128)S(1)} all-gather(f32[5,512]{1,0:T(8,128)S(1)} %psum.7), channel_id=1, replica_groups=mesh['sp'=4,'tp'=4,'dp'=2] {'tp'}, dimensions={1}, use_global_device_ids=true | all-gather | bytes 51200 | tf_op jit(solution)/shard_map/all_gather | solution.py:103
  43.7 4.2 %multiply_reduce_fusion.1 = (f32[1024]{0:T(1024)S(1)}, f32[1024,128]{0,1:T(8,128)S(1)}) fusion(bf16[2048,128]{1,0:T(8,128)(2,1)S(1)} %copy-done.22, bf16[1,1024,2048]{2,1,0:T(8,128)(2,1)} %param.15, f32[2048]{0:T(1024)S(1)} %bitcast.190, f32[2048]{0:T(1024)S(1)} %bitcast.193, f32[2048]{0:T(1024)S(1)} %copy-done.23, f32[1024]{0:T(1024)S(1)} %add_rsqrt_fusion.2), kind=kOutput, calls=%fused_computation.78 | convolution fusion | flops 549714944 | bytes 5275648 | tf_op jit(solution)/shard_map/dot_general | solution.py:124
  50.3 1.9 fusion.39
  52.8 1.9 collective-permute-start
  54.8 1.3 collective-permute-start.1
  58.1 1.8 multiply_cosine_fusion.1
  60.6 15.9 %all_gather.7 = bf16[768,256]{1,0:T(8,128)(2,1)} all-gather(bf16[192,256]{1,0:T(8,128)(2,1)S(1)} %pad_maximum_fusion.3), channel_id=1, replica_groups=mesh['sp'=4,'tp'=4,'dp'=2] {'sp'}, dimensions={0}, use_global_device_ids=true | all-gather | bytes 491520 | tf_op jit(solution)/shard_map/all_gather | solution.py:141
  76.5 4.0 %copy.51 = bf16[512,2048]{1,0:T(8,128)(2,1)} copy(bf16[512,2048]{0,1:T(8,128)(2,1)} %bitcast.180) | data formatting | bytes 4194304 | tf_op jit(solution)/shard_map/dot_general | solution.py:115
  80.5 5.4 %multiply_reduce_fusion = (f32[1024,4]{0,1:T(4,128)S(1)}, f32[1024,4,128]{0,2,1:T(8,128)S(1)}) fusion(bf16[4,128,2048]{2,1,0:T(8,128)(2,1)} %bitcast.181, bf16[1,1024,2048]{2,1,0:T(8,128)(2,1)} %param.15, f32[2048]{0:T(1024)S(1)} %bitcast.192, f32[2048]{0:T(1024)S(1)} %bitcast.195, f32[2048]{0:T(1024)S(1)} %copy-done.23, f32[1024]{0:T(1024)S(1)} %add_rsqrt_fusion.2), kind=kOutput, calls=%fused_computation.38 | convolution fusion | flops 2161111040 | bytes 8433664 | tf_op jit(solution)/shard_map/dot_general | solution.py:115
  87.4 5.6 %bitcast_reduce_fusion = (f32[4,1024]{1,0:T(4,128)S(1)}, f32[768,1024,4]{1,0,2:T(8,128)}) fusion(bf16[1024,4,32]{0,2,1:T(8,128)(2,1)S(1)} %get-tuple-element.9, bf16[1024,4,32]{0,2,1:T(8,128)(2,1)S(1)} %get-tuple-element.10, bf16[1024,4,32]{0,2,1:T(8,128)(2,1)S(1)} %get-tuple-element.6, bf16[1024,4,32]{0,2,1:T(8,128)(2,1)S(1)} %get-tuple-element.5, ...), kind=kOutput, calls=%fused_computation.1 | convolution fusion | flops 815788032 | bytes 13844480 | tf_op jit(solution)/shard_map/thgd,chd->hgtc/dot_general | solution.py:185
  93.0 1.3 broadcast_and_fusion
  95.8 1.7 copy.55
  99.7 2.4 %copy.32 = bf16[8,128,4,32]{3,1,2,0:T(8,128)(2,1)} copy(bf16[8,128,4,32]{1,0,3,2:T(8,128)(2,1)} %bitcast.188) | data formatting | bytes 524288 | tf_op jit(solution)/shard_map/concatenate | solution.py:65
  102.1 2.3 %copy.33 = bf16[8,128,4,32]{3,1,2,0:T(8,128)(2,1)} copy(bf16[8,128,4,32]{1,0,3,2:T(8,128)(2,1)} %bitcast.187) | data formatting | bytes 524288 | tf_op jit(solution)/shard_map/concatenate | solution.py:65
  104.4 1.4 copy.35
  105.8 1.4 copy.34
  107.2 1.8 pad_maximum_fusion.2
  109.1 1.2 copy.48
  111.3 1.5 pad_maximum_fusion
  113.5 3.7 %fusion.16 = (f32[4,8,128]{2,0,1:T(4,128)S(1)}, f32[8,384,128,4]{2,1,3,0:T(8,128)S(1)}) fusion(pred[8,128,384]{1,2,0:T(8,128)(4,1)S(1)} %copy-done.14, bf16[8,128,4,32]{3,1,2,0:T(8,128)(2,1)S(1)} %copy-done.5, bf16[8,128,4,32]{3,1,2,0:T(8,128)(2,1)} %copy.34, bf16[8,128,4,32]{3,1,2,0:T(8,128)(2,1)S(1)} %copy-done.4, ...), kind=kOutput, calls=%fused_computation.22 | convolution fusion | flops 411561984 | bytes 10895360 | tf_op jit(solution)/shard_map/nqhgd,nkhd->hgnqk/dot_general | solution.py:177
  117.3 2.0 %fusion.29 = f32[8,128,1,4,128]{4,1,3,0,2:T(8,128)S(1)} fusion(f32[4,8,128]{2,0,1:T(4,128)S(1)} %fusion.83, f32[8,384,128,4]{2,1,3,0:T(8,128)S(1)} %get-tuple-element.31, pred[8,128,384]{1,2,0:T(8,128)(4,1)S(1)} %copy-done.14, bf16[8,384,256]{2,1,0:T(8,128)(2,1)S(1)} %pad_maximum_fusion), kind=kOutput, calls=%fused_computation.41 | convolution fusion | flops 408944640 | bytes 9584640 | tf_op jit(solution)/shard_map/hgnqk,nkhd->nqhgd/dot_general | solution.py:198
  119.4 1.4 copy.38
  120.8 2.9 %copy.41 = f32[1024,1,4,128]{0,3,2,1:T(8,128)} copy(f32[1024,1,4,128]{3,0,2,1:T(8,128)} %bitcast.175) | data formatting | bytes 4194304 | tf_op jit(solution)/shard_map/reshape | solution.py:204
  123.8 7.7 %fusion.27 = bf16[1024,1,4,128]{0,3,2,1:T(8,128)(2,1)S(1)} fusion(f32[1024,1,4,128]{0,3,2,1:T(8,128)} %copy.41, f32[4,1024]{1,0:T(4,128)S(1)} %fusion.82, f32[768,1024,4]{1,0,2:T(8,128)} %get-tuple-element.35, bf16[768,256]{1,0:T(8,128)(2,1)S(1)} %copy-done.9), kind=kOutput, calls=%fused_computation.34 | convolution fusion | flops 815792128 | bytes 15941632 | tf_op jit(solution)/shard_map/hgtc,chd->thgd/dot_general | solution.py:201
  131.5 4.3 %convolution_convert_fusion = bf16[1024,2048]{1,0:T(8,128)(2,1)} fusion(bf16[1024,512]{0,1:T(8,128)(2,1)S(1)} %bitcast.201, bf16[512,2048]{1,0:T(8,128)(2,1)S(1)} %copy-done), kind=kOutput, calls=%fused_computation.29 | convolution fusion | flops 2149580800 | bytes 7340032 | tf_op jit(solution)/shard_map/dot_general | solution.py:210
  135.8 51.9 %reduce-scatter.2.cloned.1.call-done = bf16[256,2048]{1,0:T(8,128)(2,1)} async-done(((bf16[1024,2048]{1,0:T(8,128)(2,1)}), bf16[256,2048]{1,0:T(8,128)(2,1)}) %reduce-scatter.2.cloned.1.call-update) | async-done | bytes 1048592 | tf_op jit(solution)/shard_map/reduce_scatter | solution.py:209
  187.7 2.9 %fusion.40 = bf16[1,256,2048]{2,1,0:T(8,128)(2,1)} fusion(bf16[256,2048]{1,0:T(8,128)(2,1)} %reduce-scatter.2.cloned.1.call-done, f32[2048]{0:T(1024)S(1)} %bitcast.189, bf16[1,1024,2048]{2,1,0:T(8,128)(2,1)} %param.15, s32[]{:T(128)S(6)} %select_n.33), kind=kLoop, calls=%fused_computation.51 | loop fusion | flops 2621440 | bytes 3153924 | tf_op jit(solution)/shard_map/broadcast_in_dim | solution.py:219
  (89 shorter events, 14.5 us)
Async XLA Ops:
  6.5 124.9 %copy-start = (bf16[512,2048]{1,0:T(8,128)(2,1)S(1)}, bf16[512,2048]{1,0:T(8,128)(2,1)}, u32[]{:S(2)}) copy-start(bf16[512,2048]{1,0:T(8,128)(2,1)} %param.26) | copy-start | bytes 6291460
  6.5 37.2 %copy-start.23 = (f32[2048]{0:T(1024)S(1)}, f32[2048]{0:T(1024)}, u32[]{:S(2)}) copy-start(f32[2048]{0:T(1024)} %param.19) | copy-start | bytes 24580
  6.5 37.2 %copy-start.22 = (bf16[2048,128]{1,0:T(8,128)(2,1)S(1)}, bf16[2048,128]{1,0:T(8,128)(2,1)}, u32[]{:S(2)}) copy-start(bf16[2048,128]{1,0:T(8,128)(2,1)} %param.24) | copy-start | bytes 1572868
  6.5 181.2 %reduce-scatter.2.cloned.1.call-start = ((), (), s32[]{:S(2)}) async-start(), calls=%async_computation.1 | async-start | bytes 5242880 | tf_op jit(solution)/shard_map/reduce_scatter | solution.py:209
  43.7 4.2 %copy-start.18 = (f32[128]{0:T(128)S(1)}, f32[128]{0:T(128)}, u32[]{:S(2)}) copy-start(f32[128]{0:T(128)} %param.28) | copy-start | bytes 1540
  43.7 6.6 %copy-start.1 = (bf16[1,1024,2048]{2,1,0:T(8,128)(2,1)S(1)}, bf16[1,1024,2048]{2,1,0:T(8,128)(2,1)}, u32[]{:S(2)}) copy-start(bf16[1,1024,2048]{2,1,0:T(8,128)(2,1)} %param.15) | copy-start | bytes 12582916
  43.7 6.6 %copy-start.21 = (bf16[2048,128]{1,0:T(8,128)(2,1)S(1)}, bf16[2048,128]{1,0:T(8,128)(2,1)}, u32[]{:S(2)}) copy-start(bf16[2048,128]{1,0:T(8,128)(2,1)} %param.25) | copy-start | bytes 1572868
  50.3 6.4 %copy-start.10 = (bf16[1,192,2048]{2,1,0:T(8,128)(2,1)S(1)}, bf16[1,192,2048]{2,1,0:T(8,128)(2,1)}, u32[]{:S(2)}) copy-start(bf16[1,192,2048]{2,1,0:T(8,128)(2,1)} %param.16) | copy-start | bytes 2359300
  52.8 54.4 %collective-permute-start = (bf16[128,256]{0,1:T(8,128)(2,1)}, bf16[128,256]{0,1:T(8,128)(2,1)}, u32[]{:S(2)}, u32[]{:S(2)}) collective-permute-start(bf16[128,256]{0,1:T(8,128)(2,1)} %get-tuple-element.13), channel_id=1, source_target_pairs={{0,8},{8,16},{16,24},{1,9},{9,17},{17,25},{2,10},{10,18},{18,26},{... | collective-permute-start | bytes 196616 | tf_op jit(solution)/shard_map/ppermute | solution.py:22
  54.8 52.5 %collective-permute-start.1 = (bf16[128,256]{0,1:T(8,128)(2,1)}, bf16[128,256]{0,1:T(8,128)(2,1)}, u32[]{:S(2)}, u32[]{:S(2)}) collective-permute-start(bf16[128,256]{0,1:T(8,128)(2,1)} %get-tuple-element.14), channel_id=1, source_target_pairs={{8,0},{16,8},{24,16},{9,1},{17,9},{25,17},{10,2},{18,10},{26,18},{... | collective-permute-start | bytes 196616 | tf_op jit(solution)/shard_map/ppermute | solution.py:23
  80.5 5.5 %copy-start.20 = (f32[128]{0:T(128)S(1)}, f32[128]{0:T(128)}, u32[]{:S(2)}) copy-start(f32[128]{0:T(128)} %param.27) | copy-start | bytes 1540
  85.9 0.9 copy-start.11
  85.9 1.0 copy-start.12
  85.9 1.0 copy-start.13
  86.0 1.4 copy-start.8
  87.3 5.6 %copy-start.2 = (bf16[1024,4,32]{0,2,1:T(8,128)(2,1)}, bf16[1024,4,32]{0,2,1:T(8,128)(2,1)S(1)}, u32[]{:S(2)}) copy-start(bf16[1024,4,32]{0,2,1:T(8,128)(2,1)S(1)} %get-tuple-element.10) | copy-start | bytes 786436
  87.3 5.6 %copy-start.15 = (pred[128,384]{0,1:T(8,128)(4,1)S(1)}, pred[128,384]{0,1:T(8,128)(4,1)}, u32[]{:S(2)}) copy-start(pred[128,384]{0,1:T(8,128)(4,1)} %fusion.62) | copy-start | bytes 147460
  87.4 5.6 %copy-start.17 = (pred[8,384]{1,0:T(8,128)(4,1)S(1)}, pred[8,384]{1,0:T(8,128)(4,1)}, u32[]{:S(2)}) copy-start(pred[8,384]{1,0:T(8,128)(4,1)} %fusion.86) | copy-start | bytes 9220
  87.4 7.9 %copy-start.24 = (f32[4]{0:T(128)S(1)}, f32[4]{0:T(128)}, u32[]{:S(2)}) copy-start(f32[4]{0:T(128)} %param.29) | copy-start | bytes 52
  98.2 7.6 %copy-start.6 = (bf16[16,8,8,128]{3,2,1,0:T(8,128)(2,1)S(1)}, bf16[16,8,8,128]{3,2,1,0:T(8,128)(2,1)}, u32[]{:S(2)}) copy-start(bf16[16,8,8,128]{3,2,1,0:T(8,128)(2,1)} %copy.55) | copy-start | bytes 786436
  99.0 5.5 %copy-start.7 = (bf16[16,8,8,128]{3,2,1,0:T(8,128)(2,1)S(1)}, bf16[16,8,8,128]{3,2,1,0:T(8,128)(2,1)}, u32[]{:S(2)}) copy-start(bf16[16,8,8,128]{3,2,1,0:T(8,128)(2,1)} %copy.56) | copy-start | bytes 786436
  107.2 5.6 %copy-start.14 = (pred[8,128,384]{1,2,0:T(8,128)(4,1)S(1)}, pred[8,128,384]{1,2,0:T(8,128)(4,1)}, u32[]{:S(2)}) copy-start(pred[8,128,384]{1,2,0:T(8,128)(4,1)} %broadcast_and_fusion) | copy-start | bytes 1179652
  111.3 1.5 copy-start.3
  111.3 1.9 copy-start.4
  111.3 2.2 %copy-start.5 = (bf16[8,128,4,32]{3,1,2,0:T(8,128)(2,1)S(1)}, bf16[8,128,4,32]{3,1,2,0:T(8,128)(2,1)}, u32[]{:S(2)}) copy-start(bf16[8,128,4,32]{3,1,2,0:T(8,128)(2,1)} %copy.35) | copy-start | bytes 786436
  113.5 3.7 %copy-start.19 = (f32[4]{0:T(128)S(1)}, f32[4]{0:T(128)}, u32[]{:S(2)}) copy-start(f32[4]{0:T(128)} %exp.32) | copy-start | bytes 52
  120.8 2.9 %copy-start.9 = (bf16[768,256]{1,0:T(8,128)(2,1)S(1)}, bf16[768,256]{1,0:T(8,128)(2,1)}, u32[]{:S(2)}) copy-start(bf16[768,256]{1,0:T(8,128)(2,1)} %all_gather.7) | copy-start | bytes 1179652
  135.8 51.9 %copy-start.16 = (f32[1,2048]{1,0:T(1,128)S(1)}, f32[1,2048]{1,0:T(1,128)}, u32[]{:S(2)}) copy-start(f32[1,2048]{1,0:T(1,128)} %get-tuple-element.15) | copy-start | bytes 24580
Sparse Core Ops, SparseCore 0:
  136.0 51.7 reduce-scatter.1
where the time goes:
time: 198 us; the launch traced here: 197 us
  waiting for transfers between devices  51.9 us (26%)
  blocking collectives  44.6 us (23%)
  matrix products  39.6 us (20%)
  local copies, waits for them, and re-layouts  25.6 us (13%)
  other arithmetic  18.8 us (9%)
  between operations  13.8 us (7%)
  starting transfers between devices  3.19 us (2%)
    reduce_scatter x1, waiting for transfers between devices, per_device(): lax.psum_scatter(jnp.dot(attended, w_out, preferred_element_type=jnp.floa...  51.9 us
    psum x1, blocking collectives, per_device(): summed = lax.psum(partial_value, 'sp')  20.5 us
    all_gather x1, blocking collectives, per_device(): lax.all_gather(jnp.concatenate([piece_keys.reshape(ctx_in.shape[0], kv_wi...  15.9 us
    all_gather x1, blocking collectives, per_device(): modulation = lax.all_gather(summed, 'tp', axis=1, tiled=True)  8.23 us
    dot_general x1, matrix products, per_device(): jnp.einsum('hgtc,chd->thgd', ctx_probs, ctx_values, preferred_element_typ...  7.69 us
    concatenate x4, local copies, waits for them, and re-layouts, rotate(): jnp.concatenate([rotate_half(vectors[..., :half_dim], positions // GRID_W...  7.5 us
    dot_general x1, matrix products, per_device(): jnp.einsum('thgd,chd->hgtc', flat_queries, ctx_keys, preferred_element_ty...  5.58 us
    dot_general x1, matrix products, per_device(): jnp.dot(lat_in, w_query, preferred_element_type=jnp.float32)  5.41 us
  transfers between devices with their start and end apart: 3, of which 1 were waited for; matrix products, arithmetic and copies ran while one was open for 17% of the time, Pallas kernels for 0%

commit v1 on v0

v1 whole, which is shorter than its diff:
```python
import functools
import math

import jax
import jax.numpy as jnp
from jax import lax
from jax.experimental import pallas as pl
from jax.experimental.pallas import tpu as pltpu
from jax.sharding import PartitionSpec as P

HEAD_DIM = 128
WINDOW = 128
GRID_W = 64
NORM_EPSILON = 1e-06
ROPE_BASE = 10000.0
SLICES = 2

F32 = jnp.float32
BF16 = jnp.bfloat16


def rows_rsqrt(x):
    mean = jnp.mean(x * x, axis=-1, keepdims=True)
    return lax.rsqrt(mean + NORM_EPSILON)


def dot(a, b):
    return jnp.dot(a, b, preferred_element_type=F32)


def dot_t(a, b):
    return lax.dot_general(a, b, (((1,), (1,)), ((), ())), preferred_element_type=F32)


def body(
    n_sp,
    n_tp,
    n_dp,
    active_ref,
    gain_ref,
    qg_ref,
    kg_ref,
    sink_ref,
    latent_hbm,
    context_hbm,
    shift_hbm,
    scale_hbm,
    gate_hbm,
    wq_hbm,
    wk_hbm,
    wv_hbm,
    wo_hbm,
    out_hbm,
    lat,
    ctx,
    mods,
    wqkv,
    wfull,
    mslot,
    mfull,
    rms,
    cosb,
    sinb,
    xin,
    qbuf,
    kvbuf,
    ctxbuf,
    bias,
    att,
    arecv,
    outv,
    lsem,
    osem,
    m1s,
    m1r,
    m2s,
    m2r,
    cs,
    cr,
    hs,
    hr,
    as_,
    ar,
    ws,
    wr,
):
    sp = lax.axis_index("sp")
    tp = lax.axis_index("tp")
    dp = lax.axis_index("dp")
    tokens, width = lat.shape
    ctx_rows = ctx.shape[0]
    slot_rows = ctxbuf.shape[0] // n_sp
    mod_cols = mods.shape[2]
    qw = wq_hbm.shape[1]
    kw = wk_hbm.shape[1]
    q_local = qw // HEAD_DIM
    sub_rows = tokens // n_tp
    per_dest = sub_rows // WINDOW
    chunk = xin.shape[0]
    n_chunks = tokens // chunk
    group_rows = wo_hbm.shape[0]
    half = group_rows // n_dp
    piece = half // SLICES

    def local(src, dst, i):
        return pltpu.make_async_copy(src, dst, lsem.at[i])

    loads = [
        local(shift_hbm, mods.at[0], 0),
        local(scale_hbm, mods.at[1], 1),
        local(gate_hbm, mods.at[2], 2),
        local(latent_hbm.at[0], lat, 3),
        local(context_hbm.at[0], ctx, 4),
        local(wk_hbm, wqkv.at[:, qw : qw + kw], 5),
        local(wv_hbm, wqkv.at[:, qw + kw : qw + 2 * kw], 6),
        local(wq_hbm, wqkv.at[:, 0:qw], 7),
        local(wo_hbm, wfull.at[tp], 8),
    ]
    for load in loads:
        load.start()

    kvbuf[0:WINDOW, :] = jnp.zeros((WINDOW, kvbuf.shape[1]), BF16)
    kvbuf[tokens + WINDOW : tokens + 2 * WINDOW, :] = jnp.zeros((WINDOW, kvbuf.shape[1]), BF16)
    kvbuf[:, 2 * HEAD_DIM :] = jnp.ones((kvbuf.shape[0], HEAD_DIM), BF16)
    ctxbuf[:, 2 * HEAD_DIM :] = jnp.ones((ctxbuf.shape[0], HEAD_DIM), BF16)
    mslot[0] = jnp.zeros(mslot.shape[1:], F32)

    barrier = pltpu.get_barrier_semaphore()
    for k in range(1, n_sp):
        pl.semaphore_signal(barrier, inc=1, device_id={"sp": lax.rem(sp + k, n_sp)}, device_id_type=pl.DeviceIdType.MESH)
    for k in range(1, n_tp):
        pl.semaphore_signal(barrier, inc=1, device_id={"tp": lax.rem(tp + k, n_tp)}, device_id_type=pl.DeviceIdType.MESH)
    for k in range(1, n_dp):
        pl.semaphore_signal(barrier, inc=1, device_id={"dp": lax.rem(dp + k, n_dp)}, device_id_type=pl.DeviceIdType.MESH)

    def remote(src, dst, s_sem, r_sem, axis, index):
        return pltpu.make_async_remote_copy(
            src_ref=src,
            dst_ref=dst,
            send_sem=s_sem,
            recv_sem=r_sem,
            device_id={axis: index},
            device_id_type=pl.DeviceIdType.MESH,
        )

    act = active_ref[...]
    for i in range(3):
        loads[i].wait()
        mslot[0, 2 * i : 2 * i + 2, :] = dot(act, mods[i])[0:2, :]
    pl.semaphore_wait(barrier, n_sp + n_tp + n_dp - 3)

    phase1 = [
        remote(mslot.at[0], mslot.at[k], m1s.at[k - 1], m1r.at[k - 1], "sp", lax.rem(sp + k, n_sp))
        for k in range(1, n_sp)
    ]
    for c in phase1:
        c.start()

    lane = lax.broadcasted_iota(jnp.int32, (GRID_W, HEAD_DIM), 1)
    sub = lax.broadcasted_iota(jnp.int32, (GRID_W, HEAD_DIM), 0)
    quarter = HEAD_DIM // 4
    freq = jnp.exp((lane % quarter).astype(F32) * (-math.log(ROPE_BASE) / quarter))
    sign = jnp.where(lane % (2 * quarter) < quarter, -1.0, 1.0)
    col_ang = sub.astype(F32) * freq
    col_cos, col_sin = jnp.cos(col_ang), jnp.sin(col_ang) * sign
    n_rows = tokens // GRID_W
    row_ang = (sp * n_rows + lax.broadcasted_iota(jnp.int32, (n_rows, HEAD_DIM), 0)).astype(F32) * freq[0:1]
    row_cos, row_sin = jnp.cos(row_ang), jnp.sin(row_ang) * sign[0:1]
    for g in range(n_rows):
        cosb[g * GRID_W : (g + 1) * GRID_W, :] = jnp.where(lane < 2 * quarter, row_cos[g : g + 1], col_cos)
        sinb[g * GRID_W : (g + 1) * GRID_W, :] = jnp.where(lane < 2 * quarter, row_sin[g : g + 1], col_sin)
    off = lax.broadcasted_iota(jnp.int32, (WINDOW, 3 * WINDOW), 1) - lax.broadcasted_iota(
        jnp.int32, (WINDOW, 3 * WINDOW), 0
    )
    bias[...] = jnp.where((off >= 0) & (off <= 2 * WINDOW), 0.0, -1e30)

    for c in phase1:
        c.wait()
    total = mslot[0]
    for k in range(1, n_sp):
        total = total + mslot[k]
    mfull[tp] = total
    phase2 = [
        remote(mfull.at[tp], mfull.at[tp], m2s.at[k - 1], m2r.at[k - 1], "tp", lax.rem(tp + k, n_tp))
        for k in range(1, n_tp)
    ]
    for c in phase2:
        c.start()

    near = tp + 1 - 2 * lax.rem(tp, 2)
    far = lax.rem(tp + 2, n_tp)
    diag = near + far - tp
    first = near + dp * (far - near)
    second = far + dp * (near - far)
    mate = lax.rem(dp + 1, n_dp)

    def wrows(core, j):
        return pl.ds(pl.multiple_of(core * half + j * piece, piece), piece)

    def wcopy(kind, j, src, slot, axis, index):
        i = kind * SLICES + j
        return remote(src, wfull.at[slot, wrows(dp, j), :], ws.at[i], wr.at[i], axis, index)

    own_first = [wcopy(0, j, wo_hbm.at[wrows(dp, j), :], tp, "tp", first) for j in range(SLICES)]
    own_second = [wcopy(1, j, wo_hbm.at[wrows(dp, j), :], tp, "tp", second) for j in range(SLICES)]

    def passed(kind, j, slot, axis, index):
        return wcopy(kind, j, wfull.at[slot, wrows(dp, j), :], slot, axis, index)

    relay = [passed(2, j, first, "tp", second) for j in range(SLICES)]
    share = [
        [passed(3 + i, j, slot, "dp", mate) for j in range(SLICES)]
        for i, slot in enumerate((first, second, diag))
    ]
    for j in range(SLICES):
        own_first[j].start()
        own_second[j].start()

    loads[3].wait()

    @pl.loop(0, tokens // 32)
    def _(i):
        rows = pl.ds(pl.multiple_of(i * 32, 32), 32)
        x = lat[rows, :].astype(F32)
        rms[rows, :] = jnp.broadcast_to(rows_rsqrt(x), (32, HEAD_DIM))

    for i in (4, 5, 6):
        loads[i].wait()
    x = ctx[...].astype(F32)
    ctx_r = rows_rsqrt(x)
    for c in phase2:
        c.wait()

    def mod_row(r):
        return jnp.concatenate([mfull[j, r : r + 1, :] for j in range(n_tp)], axis=1)

    gain = gain_ref[...]
    ctx_in = (x * ctx_r * (gain * (1.0 + mod_row(3))) + mod_row(1)).astype(BF16)
    ckv = dot(ctx_in, wqkv[:, qw : qw + 2 * kw])
    ck = ckv[:, :kw]
    kg = kg_ref[...]
    ck = ck * rows_rsqrt(ck) * kg
    if slot_rows != ctx_rows:
        ctxbuf[0:slot_rows, 0 : 2 * HEAD_DIM] = jnp.zeros((slot_rows, 2 * HEAD_DIM), BF16)
    ctxbuf[0:ctx_rows, 0:HEAD_DIM] = ck.astype(BF16)
    ctxbuf[0:ctx_rows, HEAD_DIM : 2 * HEAD_DIM] = ckv[:, kw:].astype(BF16)
    ctx_copies = [
        remote(
            ctxbuf.at[0:slot_rows, 0 : 2 * HEAD_DIM],
            ctxbuf.at[k * slot_rows : (k + 1) * slot_rows, 0 : 2 * HEAD_DIM],
            cs.at[k - 1],
            cr.at[k - 1],
            "sp",
            lax.rem(sp + k, n_sp),
        )
        for k in range(1, n_sp)
    ]
    for c in ctx_copies:
        c.start()

    loads[7].wait()
    amp = gain * (1.0 + mod_row(2))
    shift = mod_row(0)
    qg = qg_ref[...] * (HEAD_DIM**-0.5 * math.log2(math.e))
    lane_c = lax.broadcasted_iota(jnp.int32, (chunk, HEAD_DIM), 1)
    is_first = lane_c % (2 * quarter) < quarter

    up_row = tokens
    halo_up = remote(
        kvbuf.at[pl.ds(up_row, WINDOW), 0 : 2 * HEAD_DIM],
        kvbuf.at[pl.ds(0, WINDOW), 0 : 2 * HEAD_DIM],
        hs.at[0],
        hr.at[0],
        "sp",
        lax.rem(sp + 1, n_sp),
    )
    halo_down = remote(
        kvbuf.at[pl.ds(WINDOW, WINDOW), 0 : 2 * HEAD_DIM],
        kvbuf.at[pl.ds(tokens + WINDOW, WINDOW), 0 : 2 * HEAD_DIM],
        hs.at[1],
        hr.at[1],
        "sp",
        lax.rem(sp + n_sp - 1, n_sp),
    )

    @pl.loop(0, n_chunks)
    def _(c):
        base = pl.multiple_of(c * chunk, chunk)

        @pl.loop(0, chunk // 16)
        def _(i):
            src = pl.ds(pl.multiple_of(base + i * 16, 16), 16)
            r = rms[src, :]
            r = jnp.concatenate([r] * (width // HEAD_DIM), axis=1)
            y = lat[src, :].astype(F32) * r * amp + shift
            xin[pl.ds(pl.multiple_of(i * 16, 16), 16), :] = y.astype(BF16)

        y = dot(xin[...], wqkv[...])
        cos_t = cosb[pl.ds(base, chunk), :]
        sin_t = sinb[pl.ds(base, chunk), :]

        def turned(v, g):
            n = v * rows_rsqrt(v) * g
            swapped = jnp.where(
                is_first,
                pltpu.roll(n, HEAD_DIM - quarter, 1),
                pltpu.roll(n, quarter, 1),
            )
            return (n * cos_t + swapped * sin_t).astype(BF16)

        dst = pl.ds(pl.multiple_of(base + WINDOW, WINDOW), chunk)
        kvbuf[dst, 0:HEAD_DIM] = turned(y[:, qw : qw + kw], kg)
        kvbuf[dst, HEAD_DIM : 2 * HEAD_DIM] = y[:, qw + kw :].astype(BF16)
        blocks = chunk // WINDOW
        for h in range(q_local):
            q = turned(y[:, h * HEAD_DIM : (h + 1) * HEAD_DIM], qg)
            for b in range(blocks):
                qbuf[c * blocks + b, h * WINDOW : (h + 1) * WINDOW, :] = q[b * WINDOW : (b + 1) * WINDOW]

    @pl.when(sp < n_sp - 1)
    def _():
        halo_up.start()

    @pl.when(sp > 0)
    def _():
        halo_down.start()

    for c in ctx_copies:
        c.wait()

    @pl.when(sp < n_sp - 1)
    def _():
        halo_up.wait_send()
        halo_down.wait_recv()

    @pl.when(sp > 0)
    def _():
        halo_down.wait_send()
        halo_up.wait_recv()

    key_iota = lax.broadcasted_iota(jnp.int32, (1, 3 * WINDOW), 1)
    seq = tokens * n_sp
    if slot_rows != ctx_rows:
        pad_iota = lax.broadcasted_iota(jnp.int32, (1, ctxbuf.shape[0]), 1)
        pad_bias = jnp.where(pad_iota % slot_rows < ctx_rows, 0.0, -1e30)

    def send_att(j, dest):
        return remote(att.at[dest], arecv.at[tp], as_.at[j], ar.at[j], "tp", dest)

    @pl.loop(0, n_tp)
    def _(j):
        dest = lax.rem(tp + 1 + j, n_tp)

        @pl.loop(0, per_dest)
        def _(i):
            b = dest * per_dest + i
            q = qbuf[b]
            win = pl.ds(pl.multiple_of(b * WINDOW, WINDOW), 3 * WINDOW)
            key_pos = sp * tokens - WINDOW + b * WINDOW + key_iota
            edge = jnp.where((key_pos >= 0) & (key_pos < seq), 0.0, -1e30)
            s = dot_t(q, kvbuf[win, 0:HEAD_DIM])
            add = bias[...] + edge
            s = (s.reshape(q_local, WINDOW, 3 * WINDOW) + add[None]).reshape(q_local * WINDOW, 3 * WINDOW)
            p = jnp.exp2(s).astype(BF16)
            sc = dot_t(q, ctxbuf[:, 0:HEAD_DIM])
            if slot_rows != ctx_rows:
                sc = sc + pad_bias
            pc = jnp.exp2(sc).astype(BF16)
            o = dot(p, kvbuf[win, HEAD_DIM:]) + dot(pc, ctxbuf[:, HEAD_DIM:])
            for h in range(q_local):
                oh = o[h * WINDOW : (h + 1) * WINDOW]
                sink = jnp.exp(jnp.full((1, HEAD_DIM), sink_ref[h], F32))
                a = oh[:, :HEAD_DIM] / (oh[:, HEAD_DIM:] + sink)
                att[dest, pl.ds(pl.multiple_of(i * WINDOW, WINDOW), WINDOW), h * HEAD_DIM : (h + 1) * HEAD_DIM] = a.astype(BF16)

        @pl.when(j < n_tp - 1)
        def _():
            send_att(j, dest).start()

    for j in range(SLICES):
        own_first[j].wait()
        relay[j].start()
        share[0][j].start()
        own_second[j].wait()
        share[1][j].start()
    for j in range(SLICES):
        relay[j].wait()
        share[2][j].start()
    loads[8].wait()
    arecv[tp] = att[tp]
    for j in range(n_tp - 1):
        send_att(j, lax.rem(tp + 1 + j, n_tp)).wait()
    for kind in range(3):
        for j in range(SLICES):
            share[kind][j].wait()

    tile = 512 if width % 512 == 0 else width
    own = pl.ds(pl.multiple_of(tp * sub_rows, sub_rows), sub_rows)
    gate_tiles = mod_row(4)
    stores = []
    for n in range(width // tile):
        cols = slice(n * tile, (n + 1) * tile)
        acc = dot(arecv[0], wfull[0, :, cols])
        for g in range(1, n_tp):
            acc = acc + dot(arecv[g], wfull[g, :, cols])
        outv[:, cols] = (lat[own, cols].astype(F32) + gate_tiles[:, cols] * acc).astype(BF16)
        store = pltpu.make_async_copy(outv.at[:, cols], out_hbm.at[0, :, cols], osem.at[n])
        store.start()
        stores.append(store)
    for store in stores:
        store.wait()


def per_device(
    latent,
    context,
    cond,
    ctx_cond,
    norm_gain,
    mod_shift,
    mod_scale,
    mod_gate,
    w_query,
    w_key,
    w_value,
    w_out,
    q_gain,
    k_gain,
    sinks,
):
    n_sp, n_tp, n_dp = (lax.axis_size(a) for a in ("sp", "tp", "dp"))
    tokens, width = latent.shape[1:]
    ctx_rows = context.shape[1]
    part_rows, mod_cols = mod_shift.shape
    qw, kw = w_query.shape[1], w_key.shape[1]
    sub_rows = tokens // n_tp
    group_rows = w_out.shape[0]
    chunk = min(512, tokens)
    slot_rows = -(-ctx_rows // 16) * 16
    assert n_tp == 4 and n_dp == 2 and kw == HEAD_DIM
    cond_rows = jnp.stack([cond[0], ctx_cond])
    own_cond = lax.dynamic_slice_in_dim(cond_rows, lax.axis_index("sp") * part_rows, part_rows, 1)
    active = jnp.pad(jax.nn.silu(own_cond).astype(BF16), ((0, 14), (0, 0)))
    vmem = pl.BlockSpec(memory_space=pltpu.VMEM)
    hbm = pl.BlockSpec(memory_space=pl.ANY)
    dma = pltpu.SemaphoreType.DMA
    return pl.pallas_call(
        functools.partial(body, n_sp, n_tp, n_dp),
        out_shape=jax.ShapeDtypeStruct((1, sub_rows, width), BF16),
        in_specs=[vmem] * 4 + [pl.BlockSpec(memory_space=pltpu.SMEM)] + [hbm] * 9,
        out_specs=hbm,
        scratch_shapes=[
            pltpu.VMEM((tokens, width), BF16),
            pltpu.VMEM((ctx_rows, width), BF16),
            pltpu.VMEM((3, part_rows, mod_cols), BF16),
            pltpu.VMEM((width, qw + 2 * kw), BF16),
            pltpu.VMEM((n_tp, group_rows, width), BF16),
            pltpu.VMEM((n_sp, 8, mod_cols), F32),
            pltpu.VMEM((n_tp, 8, mod_cols), F32),
            pltpu.VMEM((tokens, HEAD_DIM), F32),
            pltpu.VMEM((tokens, HEAD_DIM), F32),
            pltpu.VMEM((tokens, HEAD_DIM), F32),
            pltpu.VMEM((chunk, width), BF16),
            pltpu.VMEM((tokens // WINDOW, qw // HEAD_DIM * WINDOW, HEAD_DIM), BF16),
            pltpu.VMEM((tokens + 2 * WINDOW, 3 * HEAD_DIM), BF16),
            pltpu.VMEM((n_sp * slot_rows, 3 * HEAD_DIM), BF16),
            pltpu.VMEM((WINDOW, 3 * WINDOW), F32),
            pltpu.VMEM((n_tp, sub_rows, qw), BF16),
            pltpu.VMEM((n_tp, sub_rows, qw), BF16),
            pltpu.VMEM((sub_rows, width), BF16),
            dma((9,)),
            dma((max(width // 512, 1),)),
            dma((n_sp - 1,)),
            dma((n_sp - 1,)),
            dma((n_tp - 1,)),
            dma((n_tp - 1,)),
            dma((n_sp - 1,)),
            dma((n_sp - 1,)),
            dma((2,)),
            dma((2,)),
            dma((n_tp - 1,)),
            dma((n_tp - 1,)),
            dma((6 * SLICES,)),
            dma((6 * SLICES,)),
        ],
        compiler_params=pltpu.CompilerParams(
            collective_id=0, has_side_effects=True, vmem_limit_bytes=60 * 1024 * 1024
        ),
    )(
        active,
        norm_gain[None],
        q_gain[None],
        k_gain[None],
        sinks,
        latent,
        context,
        mod_shift,
        mod_scale,
        mod_gate,
        w_query,
        w_key,
        w_value,
        w_out,
    )


def solution(mesh):
    in_specs = (
        P("dp", "sp", None),
        P("dp", "sp", None),
        P("dp", None),
        P(),
        P(),
        P("sp", "tp"),
        P("sp", "tp"),
        P("sp", "tp"),
        P(None, "tp"),
        P(None, "tp"),
        P(None, "tp"),
        P("tp", None),
        P(),
        P(),
        P("tp"),
    )
    out_specs = P("dp", ("sp", "tp"), None)
    return jax.shard_map(
        per_device, mesh=mesh, in_specs=in_specs, out_specs=out_specs, check_vma=False
    )
```

time: 198 us -> 65.5 us (0.33)
  Pallas kernels: 0 us -> 61.6 us
  waiting for transfers between devices: 51.9 us -> 0 us
  blocking collectives: 44.6 us -> 0 us
  matrix products: 39.6 us -> 0 us
  local copies, waits for them, and re-layouts: 25.6 us -> 2.92 us
  other arithmetic: 18.8 us -> 0.79 us
  between operations: 13.8 us -> 0.02 us
  starting transfers between devices: 3.19 us -> 0 us
    pallas_call x0 -> x1, Pallas kernels: none -> 61.6 us  [per_device(): pl.pallas_call(functools.partial(body, n_sp, n_tp, n_dp), out_shape=jax.S...]
    reduce_scatter x1 -> x0, waiting for transfers between devices: 51.9 us -> none  [per_device(): lax.psum_scatter(jnp.dot(attended, w_out, preferred_element_type=jnp.floa...]
    dot_general x13 -> x0, matrix products: 39.6 us -> none  [the longest x1 7.69 us: per_device(): jnp.einsum('hgtc,chd->thgd', ctx_probs, ctx_values, preferred_element_typ...]
    all_gather x2 -> x0, blocking collectives: 24.1 us -> none  [the longest x1 15.9 us: per_device(): lax.all_gather(jnp.concatenate([piece_keys.reshape(ctx_in.shape[0], kv_wi...]
    psum x1 -> x0, blocking collectives: 20.5 us -> none  [per_device(): summed = lax.psum(partial_value, 'sp')]
    concatenate x4 -> x0, local copies, waits for them, and re-layouts: 7.5 us -> none  [rotate(): jnp.concatenate([rotate_half(vectors[..., :half_dim], positions // GRID_W...]
    dot_general x1 -> x0, local copies, waits for them, and re-layouts: 3.97 us -> none  [per_device(): jnp.dot(lat_in, w_query, preferred_element_type=jnp.float32)]
    slice x4 -> x0, local copies, waits for them, and re-layouts: 3.96 us -> none  [the longest x1 1.24 us: per_device(): padded_blocks[0:block_count]]
  transfers between devices with their start and end apart: 3 -> 0, of which waited for: 1 -> 0; matrix products, arithmetic and copies ran while one was open for 17% -> 0% of each run, Pallas kernels for 0% -> 0%
where the time goes in v1:
time: 65.5 us; the launch traced here: 65.3 us
  Pallas kernels  61.6 us (94%)
  local copies, waits for them, and re-layouts  2.92 us (4%)
  other arithmetic  0.79 us (1%)
    pallas_call x1, Pallas kernels, per_device(): pl.pallas_call(functools.partial(body, n_sp, n_tp, n_dp), out_shape=jax.S...  61.6 us
    unnamed x1, local copies, waits for them, and re-layouts  2.3 us

profile of v1, /device:TPU:0, one launch (start us, length us, event | category | flops | bytes accessed | tf_op | source)
XLA Modules:
  0.0 65.3 jit_solution(5583648533965259445)
XLA Ops:
  0.0 0.8 %fusion.1 = bf16[2,512]{1,0:T(2,128)(2,1)S(1)} fusion(s32[]{:T(128)S(6)} %select_n.3, f32[1,2048]{1,0:T(1,128)} %bitcast.5, f32[1,2048]{1,0:T(1,128)} %param.17), kind=kLoop, calls=%fused_computation.4 | loop fusion | flops 6144 | bytes 18436 | tf_op jit(solution)/shard_map/convert_element_type | solution.py:443
  0.8 0.6 pad.4.active_ref
  1.4 61.6 %shard_map.145 = bf16[1,256,2048]{2,1,0:T(8,128)(2,1)} custom-call(bf16[16,512]{1,0:T(8,128)(2,1)} %pad.4.active_ref, f32[1,2048]{1,0:T(1,128)} %bitcast.4, f32[1,128]{1,0:T(1,128)} %bitcast.6, f32[1,128]{1,0:T(1,128)} %bitcast.7, f32[4]{0:T(128)} %sink_ref.1, bf16[1,1024,2048]{2,1,0:T(8,128)(2,1)} %latent_hbm.1, bf16[1,192,2048]{2,1,0:T(8,128)(2,1)} %context_hbm.1, ...), custom_call_target="tpu_custom_call" | custom-call | tf_op jit(solution)/shard_map/pallas_call | solution.py:447
  63.0 2.3 %copy.17 = bf16[1,256,2048]{2,1,0:T(8,128)(2,1)} copy(bf16[1,256,2048]{2,1,0:T(8,128)(2,1)} %shard_map.145) | data formatting | bytes 2097152

commit v2 on v1

--- a/solution.py
+++ b/solution.py
@@ -13,7 +13,8 @@
 GRID_W = 64
 NORM_EPSILON = 1e-06
 ROPE_BASE = 10000.0
-SLICES = 2
+UNITS = 8
+PASSED = 2
 
 F32 = jnp.float32
 BF16 = jnp.bfloat16
@@ -100,7 +101,8 @@
     n_chunks = tokens // chunk
     group_rows = wo_hbm.shape[0]
     half = group_rows // n_dp
-    piece = half // SLICES
+    unit = half // UNITS
+    shared_units = UNITS - 2 * PASSED
 
     def local(src, dst, i):
         return pltpu.make_async_copy(src, dst, lsem.at[i])
@@ -116,7 +118,7 @@
         local(wq_hbm, wqkv.at[:, 0:qw], 7),
         local(wo_hbm, wfull.at[tp], 8),
     ]
-    for load in loads:
+    for load in loads[:3]:
         load.start()
 
     kvbuf[0:WINDOW, :] = jnp.zeros((WINDOW, kvbuf.shape[1]), BF16)
@@ -143,10 +145,64 @@
             device_id_type=pl.DeviceIdType.MESH,
         )
 
+    near = tp + 1 - 2 * lax.rem(tp, 2)
+    far = lax.rem(tp + 2, n_tp)
+    diag = near + far - tp
+    first = near + dp * (far - near)
+    second = far + dp * (near - far)
+    core_mate = lax.rem(dp + 1, n_dp)
+    parity = lax.rem(sp, 2)
+    sp_mate = sp + 1 - 2 * parity
+    slots = (first, second, diag)
+    n_direct = PASSED + 1
+
+    def wrows(start, count):
+        return pl.ds(pl.multiple_of(dp * half + start * unit, unit), count * unit)
+
+    pieces = [wrows(parity * PASSED + j, 1) for j in range(PASSED)]
+    pieces.append(wrows(2 * PASSED, shared_units))
+    pieces += [wrows((1 - parity) * PASSED + j, 1) for j in range(PASSED)]
+
+    def wcopy(i, src, slot, rows, axis, index):
+        return remote(src, wfull.at[slot, rows, :], ws.at[i], wr.at[i], axis, index)
+
+    def passed(i, slot, rows, axis, index):
+        return wcopy(i, wfull.at[slot, rows, :], slot, rows, axis, index)
+
+    to_first = [wcopy(j, wo_hbm.at[pieces[j], :], tp, pieces[j], "tp", first) for j in range(n_direct)]
+    to_second = [
+        wcopy(n_direct + j, wo_hbm.at[pieces[j], :], tp, pieces[j], "tp", second) for j in range(n_direct)
+    ]
+    relay = [passed(2 * n_direct + j, first, pieces[j], "tp", second) for j in range(n_direct)]
+    at = 3 * n_direct
+    over = [
+        [passed(at + i * PASSED + j, slots[i], pieces[j], "sp", sp_mate) for j in range(PASSED)] for i in range(3)
+    ]
+    at += 3 * PASSED
+    share = [
+        [passed(at + i * len(pieces) + j, slots[i], pieces[j], "dp", core_mate) for j in range(len(pieces))]
+        for i in range(3)
+    ]
+
+    def arrived(copies, i, j):
+        copies[j].wait_recv()
+        if j < PASSED:
+            over[i][j].start()
+        share[i][j].start()
+
+    def direct_arrived(j):
+        to_first[j].wait_recv()
+        relay[j].start()
+        share[0][j].start()
+        to_second[j].wait_recv()
+        share[1][j].start()
+
     act = active_ref[...]
     for i in range(3):
         loads[i].wait()
         mslot[0, 2 * i : 2 * i + 2, :] = dot(act, mods[i])[0:2, :]
+    for load in loads[3:]:
+        load.start()
     pl.semaphore_wait(barrier, n_sp + n_tp + n_dp - 3)
 
     phase1 = [
@@ -155,6 +211,8 @@
     ]
     for c in phase1:
         c.start()
+    to_first[0].start()
+    to_second[0].start()
 
     lane = lax.broadcasted_iota(jnp.int32, (GRID_W, HEAD_DIM), 1)
     sub = lax.broadcasted_iota(jnp.int32, (GRID_W, HEAD_DIM), 0)
@@ -187,34 +245,9 @@
     for c in phase2:
         c.start()
 
-    near = tp + 1 - 2 * lax.rem(tp, 2)
-    far = lax.rem(tp + 2, n_tp)
-    diag = near + far - tp
-    first = near + dp * (far - near)
-    second = far + dp * (near - far)
-    mate = lax.rem(dp + 1, n_dp)
-
-    def wrows(core, j):
-        return pl.ds(pl.multiple_of(core * half + j * piece, piece), piece)
-
-    def wcopy(kind, j, src, slot, axis, index):
-        i = kind * SLICES + j
-        return remote(src, wfull.at[slot, wrows(dp, j), :], ws.at[i], wr.at[i], axis, index)
-
-    own_first = [wcopy(0, j, wo_hbm.at[wrows(dp, j), :], tp, "tp", first) for j in range(SLICES)]
-    own_second = [wcopy(1, j, wo_hbm.at[wrows(dp, j), :], tp, "tp", second) for j in range(SLICES)]
-
-    def passed(kind, j, slot, axis, index):
-        return wcopy(kind, j, wfull.at[slot, wrows(dp, j), :], slot, axis, index)
-
-    relay = [passed(2, j, first, "tp", second) for j in range(SLICES)]
-    share = [
-        [passed(3 + i, j, slot, "dp", mate) for j in range(SLICES)]
-        for i, slot in enumerate((first, second, diag))
-    ]
-    for j in range(SLICES):
-        own_first[j].start()
-        own_second[j].start()
+    for j in range(1, n_direct):
+        to_first[j].start()
+        to_second[j].start()
 
     loads[3].wait()
 
@@ -257,6 +290,7 @@
     ]
     for c in ctx_copies:
         c.start()
+    direct_arrived(0)
 
     loads[7].wait()
     amp = gain * (1.0 + mod_row(2))
@@ -283,9 +317,8 @@
         lax.rem(sp + n_sp - 1, n_sp),
     )
 
-    @pl.loop(0, n_chunks)
-    def _(c):
-        base = pl.multiple_of(c * chunk, chunk)
+    for c in range(n_chunks):
+        base = c * chunk
 
         @pl.loop(0, chunk // 16)
         def _(i):
@@ -308,7 +341,7 @@
             )
             return (n * cos_t + swapped * sin_t).astype(BF16)
 
-        dst = pl.ds(pl.multiple_of(base + WINDOW, WINDOW), chunk)
+        dst = pl.ds(base + WINDOW, chunk)
         kvbuf[dst, 0:HEAD_DIM] = turned(y[:, qw : qw + kw], kg)
         kvbuf[dst, HEAD_DIM : 2 * HEAD_DIM] = y[:, qw + kw :].astype(BF16)
         blocks = chunk // WINDOW
@@ -316,6 +349,8 @@
             q = turned(y[:, h * HEAD_DIM : (h + 1) * HEAD_DIM], qg)
             for b in range(blocks):
                 qbuf[c * blocks + b, h * WINDOW : (h + 1) * WINDOW, :] = q[b * WINDOW : (b + 1) * WINDOW]
+        if c + 1 < PASSED:
+            direct_arrived(c + 1)
 
     @pl.when(sp < n_sp - 1)
     def _():
@@ -325,6 +360,8 @@
     def _():
         halo_down.start()
 
+    for j in range(n_chunks + 1, PASSED):
+        direct_arrived(j)
     for c in ctx_copies:
         c.wait()
 
@@ -337,6 +374,10 @@
     def _():
         halo_down.wait_send()
         halo_up.wait_recv()
+
+    for j in range(PASSED):
+        over[0][j].start()
+        over[1][j].start()
 
     key_iota = lax.broadcasted_iota(jnp.int32, (1, 3 * WINDOW), 1)
     seq = tokens * n_sp
@@ -347,9 +388,8 @@
     def send_att(j, dest):
         return remote(att.at[dest], arecv.at[tp], as_.at[j], ar.at[j], "tp", dest)
 
-    @pl.loop(0, n_tp)
-    def _(j):
-        dest = lax.rem(tp + 1 + j, n_tp)
+    order = (diag, far, near, tp)
+    for j, dest in enumerate(order):
 
         @pl.loop(0, per_dest)
         def _(i):
@@ -373,26 +413,35 @@
                 a = oh[:, :HEAD_DIM] / (oh[:, HEAD_DIM:] + sink)
                 att[dest, pl.ds(pl.multiple_of(i * WINDOW, WINDOW), WINDOW), h * HEAD_DIM : (h + 1) * HEAD_DIM] = a.astype(BF16)
 
-        @pl.when(j < n_tp - 1)
-        def _():
+        if j < n_tp - 1:
             send_att(j, dest).start()
-
-    for j in range(SLICES):
-        own_first[j].wait()
-        relay[j].start()
-        share[0][j].start()
-        own_second[j].wait()
-        share[1][j].start()
-    for j in range(SLICES):
-        relay[j].wait()
-        share[2][j].start()
+        if j == 2:
+            direct_arrived(PASSED)
+
     loads[8].wait()
     arecv[tp] = att[tp]
+    for j in range(PASSED):
+        arrived(relay, 2, j)
+    for i in range(2):
+        for j in range(PASSED):
+            over[i][j].wait_recv()
+            share[i][n_direct + j].start()
+    arrived(relay, 2, PASSED)
+    for j in range(PASSED):
+        over[2][j].wait_recv()
+        share[2][n_direct + j].start()
+    for j in range(n_direct):
+        to_first[j].wait_send()
+        to_second[j].wait_send()
+        relay[j].wait_send()
+    for i in range(3):
+        for j in range(PASSED):
+            over[i][j].wait_send()
     for j in range(n_tp - 1):
-        send_att(j, lax.rem(tp + 1 + j, n_tp)).wait()
-    for kind in range(3):
-        for j in range(SLICES):
-            share[kind][j].wait()
+        send_att(j, order[j]).wait()
+    for i in range(3):
+        for j in range(len(pieces)):
+            share[i][j].wait()
 
     tile = 512 if width % 512 == 0 else width
     own = pl.ds(pl.multiple_of(tp * sub_rows, sub_rows), sub_rows)
@@ -437,7 +486,8 @@
     group_rows = w_out.shape[0]
     chunk = min(512, tokens)
     slot_rows = -(-ctx_rows // 16) * 16
-    assert n_tp == 4 and n_dp == 2 and kw == HEAD_DIM
+    n_wsem = 3 * (PASSED + 1) + 3 * PASSED + 3 * (2 * PASSED + 1)
+    assert n_sp % 2 == 0 and n_tp == 4 and n_dp == 2 and kw == HEAD_DIM
     cond_rows = jnp.stack([cond[0], ctx_cond])
     own_cond = lax.dynamic_slice_in_dim(cond_rows, lax.axis_index("sp") * part_rows, part_rows, 1)
     active = jnp.pad(jax.nn.silu(own_cond).astype(BF16), ((0, 14), (0, 0)))
@@ -480,8 +530,8 @@
             dma((2,)),
             dma((n_tp - 1,)),
             dma((n_tp - 1,)),
-            dma((6 * SLICES,)),
-            dma((6 * SLICES,)),
+            dma((n_wsem,)),
+            dma((n_wsem,)),
         ],
         compiler_params=pltpu.CompilerParams(
             collective_id=0, has_side_effects=True, vmem_limit_bytes=60 * 1024 * 1024

time: 65.5 us -> 56.5 us (0.86)
  Pallas kernels: 61.6 us -> 52.5 us
    pallas_call x1, Pallas kernels: 61.6 us -> 52.5 us  [per_device(): pl.pallas_call(functools.partial(body, n_sp, n_tp, n_dp), out_shape=jax.S...]
where the time goes in v2:
time: 56.5 us; the launch traced here: 56.2 us
  Pallas kernels  52.5 us (93%)
  local copies, waits for them, and re-layouts  2.92 us (5%)
  other arithmetic  0.79 us (1%)
    pallas_call x1, Pallas kernels, per_device(): pl.pallas_call(functools.partial(body, n_sp, n_tp, n_dp), out_shape=jax.S...  52.5 us
    unnamed x1, local copies, waits for them, and re-layouts  2.3 us

profile of v2, /device:TPU:0, one launch (start us, length us, event | category | flops | bytes accessed | tf_op | source)
XLA Modules:
  0.0 56.2 jit_solution(15426645403032995524)
XLA Ops:
  0.0 0.8 %fusion.1 = bf16[2,512]{1,0:T(2,128)(2,1)S(1)} fusion(s32[]{:T(128)S(6)} %select_n.3, f32[1,2048]{1,0:T(1,128)} %bitcast.5, f32[1,2048]{1,0:T(1,128)} %param.17), kind=kLoop, calls=%fused_computation.4 | loop fusion | flops 6144 | bytes 18436 | tf_op jit(solution)/shard_map/convert_element_type | solution.py:493
  0.8 0.6 %pad.4.active_ref = bf16[16,512]{1,0:T(8,128)(2,1)} pad(bf16[2,512]{1,0:T(2,128)(2,1)S(1)} %fusion.1, bf16[]{:T(256)} %constant.15.clone.1), padding=0_14x0_0 | pad | bytes 18434 | tf_op jit(solution)/shard_map/jit(_pad)/pad | solution.py:493
  1.4 52.5 %shard_map.145 = bf16[1,256,2048]{2,1,0:T(8,128)(2,1)} custom-call(bf16[16,512]{1,0:T(8,128)(2,1)} %pad.4.active_ref, f32[1,2048]{1,0:T(1,128)} %bitcast.4, f32[1,128]{1,0:T(1,128)} %bitcast.6, f32[1,128]{1,0:T(1,128)} %bitcast.7, f32[4]{0:T(128)} %sink_ref.1, bf16[1,1024,2048]{2,1,0:T(8,128)(2,1)} %latent_hbm.1, bf16[1,192,2048]{2,1,0:T(8,128)(2,1)} %context_hbm.1, ...), custom_call_target="tpu_custom_call" | custom-call | tf_op jit(solution)/shard_map/pallas_call | solution.py:497
  53.9 2.3 %copy.17 = bf16[1,256,2048]{2,1,0:T(8,128)(2,1)} copy(bf16[1,256,2048]{2,1,0:T(8,128)(2,1)} %shard_map.145) | data formatting | bytes 2097152
